TPU v7x, 512 devices: a 4x2x32 block of a 4x8x32 slice. The times are simulated.
512 devices in a mesh: grp: 2 (over y), sp: 32 (over z), tp: 8 (over x, core).
Axes of the slice: x: 4, y: 2, z: 32, core: 2. Of those that a mesh axis runs over, the one named last changes fastest.
The devices are a block of a 4x8x32 slice.
Arguments:
- starting_stream: bfloat16 [24576, 2048], P(('grp', 'sp'), 'tp'), parts along dimension 0, may hold values from -45 to 45
- multiplier_matrix: bfloat16 [2, 2048, 2048], P(None, 'sp', 'tp'), may hold values from -0.125 to 0.125
- memory_path_matrix: bfloat16 [2, 2048, 2048], P(None, 'sp', 'tp'), may hold values from -0.125 to 0.125
- filter_coefficients: bfloat16 [2, 4, 2048], P(None, None, 'tp'), may hold values from -3 to 3
- memory_valve_matrix: bfloat16 [2, 8, 256, 256], P(None, 'tp'), may hold values from -0.375 to 0.375
- entry_valve_matrix: bfloat16 [2, 8, 256, 256], P(None, 'tp'), may hold values from -0.375 to 0.375
- forgetting_parameters: float32 [2, 2048], P(None, 'tp'), may hold values from 3 to 15
- timestep_forgetting_multiplier: float32 [24576], P(('grp', 'sp')), parts along dimension 0, may hold values from 0.5 to 2
- spike_extra: float32 [24576, 2048], P(('grp', 'sp'), 'tp'), parts along dimension 0, may hold values from -0.7 to 0
- exit_projector_matrix: bfloat16 [2, 2048, 2048], P(None, 'tp', 'sp'), may hold values from -0.125 to 0.125
- prelude_rms_gains: float32 [2, 2048], replicated, may hold values from 0.1 to 1.9
- finishing_rms_gains: float32 [2048], P('tp'), may hold values from 0.1 to 1.9
Outputs:
- result: bfloat16 [24576, 2048], P(('grp', 'sp'), 'tp'), parts along dimension 0
There are 2 independent parts, one for each index of `grp`. A program takes and returns all parts, laid end to end along the dimension named above; an argument that names none is the same for every part. Nothing has to cross between parts.
All inputs are finite; a program needn't handle non-finite values.
Results may differ from a plain program's by a relative error of at most 0.015.
Values may be sent and summed in bfloat16 or wider, within the bound.
A program may use at most 64 MiB of HBM per device.

v0:
```python
import jax
import jax.numpy as jnp
from jax import lax
from jax.sharding import PartitionSpec as P

BLOCK_W = 256
EPSILON = 1e-06
SQUASH_POWER = 8.0


def sent_to_all(x, axis):
    copies = jnp.broadcast_to(x, (lax.axis_size(axis), *x.shape))
    return lax.all_to_all(copies, axis, split_axis=0, concat_axis=0, tiled=True)


def laid_out(tiles, dim):
    lengths = list(tiles.shape[1:])
    lengths[dim] *= tiles.shape[0]
    return jnp.moveaxis(tiles, 0, dim).reshape(lengths)


def gather_directly(x, axis, dim):
    tiles = sent_to_all(x, axis)
    return laid_out(tiles, dim)


def in_one_piece(arrays, axis, dim, along):
    widths = [a.shape[along] for a in arrays]
    both = jnp.concatenate(arrays, axis=along)
    whole = lax.all_gather(both, axis, axis=dim, tiled=True)
    return tuple(jnp.split(whole, [sum(widths[:k]) for k in range(1, len(widths))], axis=along))


def from_behind(value, axis, steps):
    count = lax.axis_size(axis)
    first, last = (max(0, -steps), min(count, count - steps))
    return lax.ppermute(value, axis, [(source, source + steps) for source in range(first, last)])


def gathered_once(x, axis):
    leaves = jax.tree.leaves(x)
    turns = sorted(range(len(leaves)), key=lambda k: -leaves[k].size)
    width = (1, *leaves[turns[0]].shape)[-1]
    lines = [
        jnp.pad(leaves[k].reshape(-1), (0, -leaves[k].size % width)).reshape(-1, width)
        for k in turns
    ]
    both, at, found = (lax.all_gather(jnp.concatenate(lines), axis), 0, {})
    for k, line in zip(turns, lines):
        slab = both[:, at : at + len(line)].reshape(len(both), -1)
        found[k] = slab[:, : leaves[k].size].reshape(-1, *leaves[k].shape)
        at += len(line)
    numbers = iter(range(len(leaves)))
    return jax.tree.map(lambda _: found[next(numbers)], x)


def carried_in(part, axis, combine, identity):
    place = lax.axis_index(axis)
    gathered = gathered_once(part, axis)
    state = jax.tree.map(lambda a, e: jnp.zeros_like(a) + jnp.asarray(e, a.dtype), part, identity)

    def one(lap, state):
        return combine(
            state, jax.tree.map(lambda a: lax.dynamic_index_in_dim(a, lap, 0, False), gathered)
        )

    return lax.fori_loop(0, place, one, state)


def split_up(x, dim, count):
    before, after = (x.shape[:dim], x.shape[dim + 1 :])
    return jnp.moveaxis(x.reshape(*before, count, -1, *after), dim, 0)


def summed_on_arrival(x, axis, dim):
    tiles = split_up(x, dim, lax.axis_size(axis))
    arrived = lax.all_to_all(tiles, axis, split_axis=0, concat_axis=0, tiled=True)
    return arrived.astype(jnp.float32).sum(axis=0)


def of_everyone(x, axis):
    everything = sent_to_all(x, axis)
    return jnp.sum(everything, axis=0)


def combine_pairs(earlier, later):
    return (earlier[0] * later[0], later[0] * earlier[1] + later[1])


def gather_rows(own_cols):
    return gather_directly(own_cols, "tp", 1)


def fetch_layer(multiplier_matrix, memory_path_matrix, exit_projector_matrix, tier_number):
    in_pair = in_one_piece(
        (multiplier_matrix[tier_number], memory_path_matrix[tier_number]), "sp", 0, 1
    )
    out_full = lax.all_gather(exit_projector_matrix[tier_number], "sp", axis=1, tiled=True)
    return (in_pair[0], in_pair[1], out_full)


def on_device(
    starting_stream,
    multiplier_matrix,
    memory_path_matrix,
    filter_coefficients,
    memory_valve_matrix,
    entry_valve_matrix,
    forgetting_parameters,
    timestep_forgetting_multiplier,
    spike_extra,
    exit_projector_matrix,
    prelude_rms_gains,
    finishing_rms_gains,
):
    tok_rows = starting_stream.shape[0]
    channels = memory_path_matrix.shape[2]
    own_cols = starting_stream
    full_rows = gather_rows(starting_stream)
    fetched = fetch_layer(multiplier_matrix, memory_path_matrix, exit_projector_matrix, 0)
    for tier_number in range(memory_path_matrix.shape[0]):
        floats = full_rows.astype(jnp.float32)
        mean_square = jnp.mean(floats * floats, axis=1, keepdims=True)
        normed = (
            floats * lax.rsqrt(mean_square + EPSILON) * prelude_rms_gains[tier_number][None, :]
        ).astype(jnp.bfloat16)
        branch_acc = jnp.dot(normed, fetched[0], preferred_element_type=jnp.float32)
        recur_acc = jnp.dot(normed, fetched[1], preferred_element_type=jnp.float32)
        out_full = fetched[2]
        if tier_number + 1 < memory_path_matrix.shape[0]:
            fetched = fetch_layer(
                multiplier_matrix, memory_path_matrix, exit_projector_matrix, tier_number + 1
            )
        branch = branch_acc.astype(jnp.bfloat16)
        recurrent = recur_acc.astype(jnp.bfloat16)
        taps_now = filter_coefficients[tier_number]
        reach_back = taps_now.shape[0] - 1
        halo_rows = from_behind(recurrent[tok_rows - reach_back :], "sp", 1)
        extended = jnp.concatenate([halo_rows, recurrent], axis=0)
        conv_sum = jnp.zeros((tok_rows, channels), jnp.float32)
        for offset in range(taps_now.shape[0]):
            conv_sum = conv_sum + extended[offset : offset + tok_rows].astype(
                jnp.float32
            ) * taps_now[offset].astype(jnp.float32)
        convolved = conv_sum.astype(jnp.bfloat16)
        blocks = convolved.reshape(tok_rows, channels // BLOCK_W, BLOCK_W)
        reset_gate = jax.nn.sigmoid(
            jnp.einsum(
                "tnc,ncd->tnd",
                blocks,
                memory_valve_matrix[tier_number],
                preferred_element_type=jnp.float32,
            ).reshape(tok_rows, channels)
        )
        inject = jax.nn.sigmoid(
            jnp.einsum(
                "tnc,ncd->tnd",
                blocks,
                entry_valve_matrix[tier_number],
                preferred_element_type=jnp.float32,
            ).reshape(tok_rows, channels)
        )
        logarithmic_persistence = (
            -SQUASH_POWER
            * reset_gate
            * jax.nn.softplus(-forgetting_parameters[tier_number])[None, :]
            * timestep_forgetting_multiplier[:, None]
            + spike_extra
        )
        keep_rate = jnp.exp(logarithmic_persistence)
        driven = (
            inject
            * convolved.astype(jnp.float32)
            * jnp.sqrt(-jnp.expm1(2.0 * logarithmic_persistence))
        )
        keep_cum, state_local = lax.associative_scan(combine_pairs, (keep_rate, driven), axis=0)
        identity = (jnp.ones((channels,), jnp.float32), jnp.zeros((channels,), jnp.float32))
        carried = carried_in((keep_cum[-1], state_local[-1]), "sp", combine_pairs, identity)
        state_seq = state_local + keep_cum * carried[1][None, :]
        mixed_in = (jax.nn.gelu(branch.astype(jnp.float32)) * state_seq).astype(jnp.bfloat16)
        partial_value = jnp.dot(mixed_in, out_full, preferred_element_type=jnp.float32)
        mixed_sum = summed_on_arrival(partial_value.astype(jnp.bfloat16), "tp", 1)
        own_cols = (own_cols.astype(jnp.float32) + mixed_sum).astype(jnp.bfloat16)
        if tier_number + 1 < memory_path_matrix.shape[0]:
            full_rows = gather_rows(own_cols)
    floats = own_cols.astype(jnp.float32)
    full_width = floats.shape[1] * lax.axis_size("tp")
    square_sum = of_everyone(jnp.sum(floats * floats, axis=1), "tp")
    inv_rms = lax.rsqrt(square_sum / full_width + EPSILON)
    return (floats * inv_rms[:, None] * finishing_rms_gains[None, :]).astype(jnp.bfloat16)


def solution(mesh):
    return jax.shard_map(
        on_device,
        mesh=mesh,
        in_specs=(
            P(("grp", "sp"), "tp"),
            P(None, "sp", "tp"),
            P(None, "sp", "tp"),
            P(None, None, "tp"),
            P(None, "tp", None, None),
            P(None, "tp", None, None),
            P(None, "tp"),
            P(("grp", "sp")),
            P(("grp", "sp"), "tp"),
            P(None, "tp", "sp"),
            P(),
            P("tp"),
        ),
        out_specs=P(("grp", "sp"), "tp"),
        check_vma=False,
    )
```

profile of v0, /device:TPU:33, one launch (start us, length us, event | category | flops | bytes accessed | tf_op | source)
XLA Modules:
  0.0 602.2 jit_solution(12787368369105031495)
XLA Ops:
  6.6 0.8 slice_bitcast_fusion
  8.1 1.4 fusion.135
  9.6 1.1 copy.23
  10.7 1.3 broadcast_in_dim.6
  12.0 45.1 %all-to-all-start = ((bf16[8,384,256]{1,2,0:T(8,128)(2,1)}), bf16[8,384,256]{1,2,0:T(8,128)(2,1)S(1)}, u32[]{:S(2)}, u32[]{:S(2)}) async-start(bf16[8,384,256]{1,2,0:T(8,128)(2,1)} %broadcast_in_dim.6), calls=%async_computation | async-start | bytes 3145728 | tf_op jit(solution)/shard_map/all_to_all | solution.py:13
  59.1 18.7 %all-to-all-done = bf16[8,384,256]{1,2,0:T(8,128)(2,1)S(1)} async-done(((bf16[8,384,256]{1,2,0:T(8,128)(2,1)}), bf16[8,384,256]{1,2,0:T(8,128)(2,1)S(1)}, u32[]{:S(2)}, u32[]{:S(2)}) %all-to-all-start) | async-done | bytes 1572896 | tf_op jit(solution)/shard_map/all_to_all | solution.py:13
  78.6 72.2 %all-gather.11.cloned.1.call-done = bf16[2048,512]{1,0:T(8,128)(2,1)} async-done(((bf16[64,512]{1,0:T(8,128)(2,1)}), bf16[2048,512]{1,0:T(8,128)(2,1)}) %all-gather.11.cloned.1.call-update) | async-done | bytes 2097168 | tf_op jit(solution)/shard_map/all_gather | solution.py:30
  150.8 1.8 convolution_convert_fusion.4
  152.7 1.7 collective-permute-start
  174.2 1.5 pad.227
  177.4 40.9 %all-gather.4 = f32[32,2,256]{2,1,0:T(2,128)S(1)} all-gather(f32[1,2,256]{2,1,0:T(2,128)S(1)} %maximum_bitcast_fusion), channel_id=2, replica_groups=mesh['grp'=2,'sp'=32,'tp'=8] {'sp'}, dimensions={0}, use_global_device_ids=true | all-gather | bytes 67584 | tf_op jit(solution)/shard_map/all_gather | solution.py:48
  218.4 59.8 %all-gather.15.cloned.1.call-done = bf16[1,256,2048]{1,2,0:T(8,128)(2,1)} async-done(((bf16[1,256,64]{1,2,0:T(8,128)(2,1)}), bf16[1,256,2048]{1,2,0:T(8,128)(2,1)}) %all-gather.15.cloned.1.call-update) | async-done | bytes 1048592 | tf_op jit(solution)/shard_map/all_gather | solution.py:98
  278.2 3.8 convolution_convert_fusion.1
  282.1 46.2 %all_to_all.26 = bf16[8,384,256]{2,1,0:T(8,128)(2,1)S(1)} all-to-all(bf16[8,384,256]{2,1,0:T(8,128)(2,1)S(1)} %bitcast.108), channel_id=1, replica_groups=mesh['grp'=2,'sp'=32,'tp'=8] {'tp'}, dimensions={0} | all-to-all | bytes 3145728 | tf_op jit(solution)/shard_map/all_to_all | solution.py:77
  329.5 1.3 broadcast_in_dim.7
  330.8 4.5 all-to-all-start.2
  335.9 20.1 %all-to-all-done.2 = bf16[8,384,256]{1,2,0:T(8,128)(2,1)S(1)} async-done(((bf16[8,384,256]{1,2,0:T(8,128)(2,1)}), bf16[8,384,256]{1,2,0:T(8,128)(2,1)S(1)}, u32[]{:S(2)}, u32[]{:S(2)}) %all-to-all-start.2) | async-done | bytes 1572896 | tf_op jit(solution)/shard_map/all_to_all | solution.py:13
  356.9 52.8 %all-gather.13.cloned.1.call-done = bf16[2048,512]{1,0:T(8,128)(2,1)} async-done(((bf16[64,512]{1,0:T(8,128)(2,1)}), bf16[2048,512]{1,0:T(8,128)(2,1)}) %all-gather.13.cloned.1.call-update) | async-done | bytes 2097168 | tf_op jit(solution)/shard_map/all_gather | solution.py:30
  409.7 1.8 convolution_convert_fusion.2
  411.6 1.5 collective-permute-start.1
  414.2 1.3 fusion.22
  415.9 0.8 slice.719
  416.7 1.0 multiply_add_fusion.2
  440.9 0.8 fusion.105
  443.3 1.6 pad.259
  446.4 1.7 pad.242
  448.8 41.6 %all-gather.5 = f32[32,2,256]{2,1,0:T(2,128)S(1)} all-gather(f32[1,2,256]{2,1,0:T(2,128)S(1)} %maximum_bitcast_fusion.1), channel_id=4, replica_groups=mesh['grp'=2,'sp'=32,'tp'=8] {'sp'}, dimensions={0}, use_global_device_ids=true | all-gather | bytes 67584 | tf_op jit(solution)/shard_map/all_gather | solution.py:48
  490.5 45.1 %all-gather.17.cloned.1.call-done = bf16[1,256,2048]{1,2,0:T(8,128)(2,1)} async-done(((bf16[1,256,64]{1,2,0:T(8,128)(2,1)}), bf16[1,256,2048]{1,2,0:T(8,128)(2,1)}) %all-gather.17.cloned.1.call-update) | async-done | bytes 1048592 | tf_op jit(solution)/shard_map/all_gather | solution.py:98
  535.7 3.9 convolution_convert_fusion
  539.7 46.7 %all_to_all.27 = bf16[8,384,256]{2,1,0:T(8,128)(2,1)S(1)} all-to-all(bf16[8,384,256]{2,1,0:T(8,128)(2,1)S(1)} %bitcast.109), channel_id=1, replica_groups=mesh['grp'=2,'sp'=32,'tp'=8] {'tp'}, dimensions={0} | all-to-all | bytes 3145728 | tf_op jit(solution)/shard_map/all_to_all | solution.py:77
  586.7 8.1 %all_to_all.28 = f32[8,1,384]{2,1,0:T(1,128)S(1)} all-to-all(f32[8,1,384]{2,1,0:T(1,128)S(1)} %broadcast_in_dim.8), channel_id=1, replica_groups=mesh['grp'=2,'sp'=32,'tp'=8] {'tp'}, dimensions={0} | all-to-all | bytes 24576 | tf_op jit(solution)/shard_map/all_to_all | solution.py:13
  594.9 0.8 fusion.36
  (388 shorter events, 55.8 us)
Async XLA Ops:
  6.5 144.2 %all-gather.11.cloned.1.call-start = ((), (), s32[]{:S(2)}) async-start(), calls=%async_computation.5 | async-start | bytes 2162688 | tf_op jit(solution)/shard_map/all_gather | solution.py:30
  8.1 270.1 %all-gather.15.cloned.1.call-start = ((), (), s32[]{:S(2)}) async-start(), calls=%async_computation.7 | async-start | bytes 1081344 | tf_op jit(solution)/shard_map/all_gather | solution.py:98
  12.0 45.8 %copy-start.28 = (f32[2,256]{1,0:T(2,128)S(1)}, f32[2,256]{1,0:T(2,128)}, u32[]{:S(2)}) copy-start(f32[2,256]{1,0:T(2,128)} %param.22) | copy-start | bytes 6148
  12.0 46.4 %copy-start.11 = (bf16[2,4,256]{2,1,0:T(4,128)(2,1)S(1)}, bf16[2,4,256]{2,1,0:T(4,128)(2,1)}, u32[]{:S(2)}) copy-start(bf16[2,4,256]{2,1,0:T(4,128)(2,1)} %param.19) | copy-start | bytes 12292
  12.0 47.0 %copy-start.10 = (f32[2,2048]{1,0:T(2,128)S(1)}, f32[2,2048]{1,0:T(2,128)}, u32[]{:S(2)}) copy-start(f32[2,2048]{1,0:T(2,128)} %param.26) | copy-start | bytes 49156
  12.0 65.7 %all-to-all-start = ((bf16[8,384,256]{1,2,0:T(8,128)(2,1)}), bf16[8,384,256]{1,2,0:T(8,128)(2,1)S(1)}, u32[]{:S(2)}, u32[]{:S(2)}) async-start(bf16[8,384,256]{1,2,0:T(8,128)(2,1)} %broadcast_in_dim.6), calls=%async_computation | async-start | bytes 3145728 | tf_op jit(solution)/shard_map/all_to_all | solution.py:13
  57.1 352.6 %all-gather.13.cloned.1.call-start = ((), (), s32[]{:S(2)}) async-start(), calls=%async_computation.6 | async-start | bytes 2162688 | tf_op jit(solution)/shard_map/all_gather | solution.py:30
  78.6 76.7 %copy-start.31 = (f32[384,256]{1,0:T(8,128)S(1)}, f32[384,256]{1,0:T(8,128)}, u32[]{:S(2)}) copy-start(f32[384,256]{1,0:T(8,128)} %param.24) | copy-start | bytes 1179652
  78.6 76.7 %copy-start.33 = (bf16[2,1,256,256]{3,2,1,0:T(8,128)(2,1)S(1)}, bf16[2,1,256,256]{3,2,1,0:T(8,128)(2,1)}, u32[]{:S(2)}) copy-start(bf16[2,1,256,256]{3,2,1,0:T(8,128)(2,1)} %param.20) | copy-start | bytes 786436
  78.6 76.7 %copy-start.36 = (f32[384]{0:T(512)S(1)}, f32[384]{0:T(512)}, u32[]{:S(2)}) copy-start(f32[384]{0:T(512)} %param.23) | copy-start | bytes 4612
  152.7 2.5 collective-permute-start
  156.1 11.2 %copy-start = (f32[384,256]{1,0:T(8,128)}, f32[384,256]{1,0:T(8,128)S(1)}, u32[]{:S(2)}) copy-start(f32[384,256]{1,0:T(8,128)S(1)} %fusion.25) | copy-start | bytes 1179652
  176.5 101.7 %copy-start.5 = (f32[384,256]{1,0:T(8,128)}, f32[384,256]{1,0:T(8,128)S(1)}, u32[]{:S(2)}) copy-start(f32[384,256]{1,0:T(8,128)S(1)} %pad.226) | copy-start | bytes 1179652
  177.2 101.0 %copy-start.6 = (f32[384,256]{1,0:T(8,128)}, f32[384,256]{1,0:T(8,128)S(1)}, u32[]{:S(2)}) copy-start(f32[384,256]{1,0:T(8,128)S(1)} %pad.211) | copy-start | bytes 1179652
  330.8 25.2 %all-to-all-start.2 = ((bf16[8,384,256]{1,2,0:T(8,128)(2,1)}), bf16[8,384,256]{1,2,0:T(8,128)(2,1)S(1)}, u32[]{:S(2)}, u32[]{:S(2)}) async-start(bf16[8,384,256]{1,2,0:T(8,128)(2,1)} %broadcast_in_dim.7), calls=%async_computation.2 | async-start | bytes 3145728 | tf_op jit(solution)/shard_map/all_to_all | solution.py:13
  335.3 200.3 %all-gather.17.cloned.1.call-start = ((), (), s32[]{:S(2)}) async-start(), calls=%async_computation.8 | async-start | bytes 1081344 | tf_op jit(solution)/shard_map/all_gather | solution.py:98
  356.8 56.7 %copy-start.12 = (f32[1,1,256]{2,1,0:T(1,128)S(1)}, f32[1,1,256]{2,1,0:T(1,128)}, u32[]{:S(2)}) copy-start(f32[1,1,256]{2,1,0:T(1,128)} %get-tuple-element.193) | copy-start | bytes 3076
  356.9 56.7 %copy-start.13 = (f32[1,1,256]{2,1,0:T(1,128)S(1)}, f32[1,1,256]{2,1,0:T(1,128)}, u32[]{:S(2)}) copy-start(f32[1,1,256]{2,1,0:T(1,128)} %get-tuple-element.194) | copy-start | bytes 3076
  356.9 56.7 %copy-start.14 = (f32[1,1,256]{2,1,0:T(1,128)S(1)}, f32[1,1,256]{2,1,0:T(1,128)}, u32[]{:S(2)}) copy-start(f32[1,1,256]{2,1,0:T(1,128)} %get-tuple-element.199) | copy-start | bytes 3076
  356.9 56.7 %copy-start.15 = (f32[1,1,256]{2,1,0:T(1,128)S(1)}, f32[1,1,256]{2,1,0:T(1,128)}, u32[]{:S(2)}) copy-start(f32[1,1,256]{2,1,0:T(1,128)} %get-tuple-element.200) | copy-start | bytes 3076
  356.9 56.9 %copy-start.30 = (f32[1,256]{1,0:T(1,128)S(1)}, f32[1,256]{1,0:T(1,128)}, u32[]{:S(2)}) copy-start(f32[1,256]{1,0:T(1,128)} %get-tuple-element.209) | copy-start | bytes 3076
  356.9 56.9 %copy-start.32 = (f32[384,256]{1,0:T(8,128)S(1)}, f32[384,256]{1,0:T(8,128)}, u32[]{:S(2)}) copy-start(f32[384,256]{1,0:T(8,128)} %param.24) | copy-start | bytes 1179652
  356.9 56.9 %copy-start.34 = (bf16[2,1,256,256]{3,2,1,0:T(8,128)(2,1)S(1)}, bf16[2,1,256,256]{3,2,1,0:T(8,128)(2,1)}, u32[]{:S(2)}) copy-start(bf16[2,1,256,256]{3,2,1,0:T(8,128)(2,1)} %param.20) | copy-start | bytes 786436
  356.9 56.9 %copy-start.37 = (f32[384]{0:T(512)S(1)}, f32[384]{0:T(512)}, u32[]{:S(2)}) copy-start(f32[384]{0:T(512)} %param.23) | copy-start | bytes 4612
  411.6 2.0 collective-permute-start.1
  415.5 18.7 %copy-start.1 = (f32[384,256]{1,0:T(8,128)}, f32[384,256]{1,0:T(8,128)S(1)}, u32[]{:S(2)}) copy-start(f32[384,256]{1,0:T(8,128)S(1)} %fusion.22) | copy-start | bytes 1179652
  432.5 8.2 %copy-start.25 = (f32[1,256]{1,0:T(1,128)S(1)}, f32[1,256]{1,0:T(1,128)}, u32[]{:S(2)}) copy-start(f32[1,256]{1,0:T(1,128)} %slice.887) | copy-start | bytes 3076
  432.5 8.3 %copy-start.23 = (f32[1,256]{1,0:T(1,128)S(1)}, f32[1,256]{1,0:T(1,128)}, u32[]{:S(2)}) copy-start(f32[1,256]{1,0:T(1,128)} %slice.861) | copy-start | bytes 3076
  432.5 8.4 %copy-start.7 = (f32[47,256]{1,0:T(8,128)S(1)}, f32[47,256]{1,0:T(8,128)}, u32[]{:S(2)}) copy-start(f32[47,256]{1,0:T(8,128)} %slice.769) | copy-start | bytes 144388
  445.6 90.0 %copy-start.3 = (f32[384,256]{1,0:T(8,128)}, f32[384,256]{1,0:T(8,128)S(1)}, u32[]{:S(2)}) copy-start(f32[384,256]{1,0:T(8,128)S(1)} %pad.258) | copy-start | bytes 1179652
  446.4 89.3 %copy-start.4 = (f32[384,256]{1,0:T(8,128)}, f32[384,256]{1,0:T(8,128)S(1)}, u32[]{:S(2)}) copy-start(f32[384,256]{1,0:T(8,128)S(1)} %pad.243) | copy-start | bytes 1179652
  586.3 8.5 %copy-start.29 = (f32[256]{0:T(256)S(1)}, f32[256]{0:T(256)}, u32[]{:S(2)}) copy-start(f32[256]{0:T(256)} %param.27) | copy-start | bytes 3076
  (16 other events, 60.6 us)
Sparse Core Ops, SparseCore 0:
  9.4 141.3 all-gather.10
  152.9 125.2 all-gather.14
  280.3 129.3 all-gather.12
  411.6 123.9 all-gather.16
where the time goes:
time: 604 us; the launch traced here: 602 us
  waiting for transfers between devices  271 us (45%)
  blocking collectives  183 us (30%)
  starting transfers between devices  52.9 us (9%)
  local copies, waits for them, and re-layouts  42.2 us (7%)
  other arithmetic  24.4 us (4%)
  between operations  14.8 us (2%)
  matrix products  13.7 us (2%)
    all_gather x2, waiting for transfers between devices, in_one_piece(): whole = lax.all_gather(both, axis, axis=dim, tiled=True)  125 us
    all_gather x2, waiting for transfers between devices, fetch_layer(): lax.all_gather(exit_projector_matrix[tier_number], 'sp', axis=1, tiled=True)  105 us
    all_to_all x2, blocking collectives, summed_on_arrival(): lax.all_to_all(tiles, axis, split_axis=0, concat_axis=0, tiled=True)  92.9 us
    all_gather x2, blocking collectives, gathered_once(): both, at, found = (lax.all_gather(jnp.concatenate(lines), axis), 0, {})  82.5 us
    all_to_all x2, starting transfers between devices, sent_to_all(): return lax.all_to_all(copies, axis, split_axis=0, concat_axis=0, tiled=True)  49.6 us
    all_to_all x2, waiting for transfers between devices, sent_to_all(): return lax.all_to_all(copies, axis, split_axis=0, concat_axis=0, tiled=True)  38.8 us
    slice x114, local copies, waits for them, and re-layouts, on_device(): lax.associative_scan(combine_pairs, (keep_rate, driven), axis=0)  28.4 us
  transfers between devices with their start and end apart: 8, of which 8 were waited for; matrix products, arithmetic and copies ran while one was open for 12% of the time, Pallas kernels for 0%

commit v1 on v0

--- a/solution.py
+++ b/solution.py
@@ -95,7 +95,7 @@
     in_pair = in_one_piece(
         (multiplier_matrix[tier_number], memory_path_matrix[tier_number]), "sp", 0, 1
     )
-    out_full = lax.all_gather(exit_projector_matrix[tier_number], "sp", axis=1, tiled=True)
+    out_full = jnp.concatenate(lax.all_gather(exit_projector_matrix[tier_number], "sp"), axis=1)
     return (in_pair[0], in_pair[1], out_full)
 
 

time: 604 us -> 604 us (level)
  no operation moved by 1% of the time
where the time goes in v1:
time: 604 us; the launch traced here: 602 us
  waiting for transfers between devices  271 us (45%)
  blocking collectives  183 us (30%)
  starting transfers between devices  52.9 us (9%)
  local copies, waits for them, and re-layouts  42.2 us (7%)
  other arithmetic  24.4 us (4%)
  between operations  14.8 us (2%)
  matrix products  13.7 us (2%)
    all_gather x2, waiting for transfers between devices, in_one_piece(): whole = lax.all_gather(both, axis, axis=dim, tiled=True)  125 us
    all_gather x2, waiting for transfers between devices, fetch_layer(): lax.all_gather(exit_projector_matrix[tier_number], 'sp')  105 us
    all_to_all x2, blocking collectives, summed_on_arrival(): lax.all_to_all(tiles, axis, split_axis=0, concat_axis=0, tiled=True)  92.9 us
    all_gather x2, blocking collectives, gathered_once(): both, at, found = (lax.all_gather(jnp.concatenate(lines), axis), 0, {})  82.5 us
    all_to_all x2, starting transfers between devices, sent_to_all(): return lax.all_to_all(copies, axis, split_axis=0, concat_axis=0, tiled=True)  49.6 us
    all_to_all x2, waiting for transfers between devices, sent_to_all(): return lax.all_to_all(copies, axis, split_axis=0, concat_axis=0, tiled=True)  38.8 us
    slice x114, local copies, waits for them, and re-layouts, on_device(): lax.associative_scan(combine_pairs, (keep_rate, driven), axis=0)  28.4 us
  transfers between devices with their start and end apart: 8, of which 8 were waited for; matrix products, arithmetic and copies ran while one was open for 12% of the time, Pallas kernels for 0%

profile of v1, /device:TPU:33, one launch (start us, length us, event | category | flops | bytes accessed | tf_op | source)
XLA Modules:
  0.0 602.2 jit_solution(12787368369105031495)
XLA Ops:
  6.6 0.8 slice_bitcast_fusion
  8.1 1.4 fusion.133
  9.6 1.1 copy.23
  10.7 1.3 broadcast_in_dim.6
  12.0 45.1 %all-to-all-start = ((bf16[8,384,256]{1,2,0:T(8,128)(2,1)}), bf16[8,384,256]{1,2,0:T(8,128)(2,1)S(1)}, u32[]{:S(2)}, u32[]{:S(2)}) async-start(bf16[8,384,256]{1,2,0:T(8,128)(2,1)} %broadcast_in_dim.6), calls=%async_computation | async-start | bytes 3145728 | tf_op jit(solution)/shard_map/all_to_all | solution.py:13
  59.1 18.7 %all-to-all-done = bf16[8,384,256]{1,2,0:T(8,128)(2,1)S(1)} async-done(((bf16[8,384,256]{1,2,0:T(8,128)(2,1)}), bf16[8,384,256]{1,2,0:T(8,128)(2,1)S(1)}, u32[]{:S(2)}, u32[]{:S(2)}) %all-to-all-start) | async-done | bytes 1572896 | tf_op jit(solution)/shard_map/all_to_all | solution.py:13
  78.6 72.2 %all-gather.9.cloned.1.call-done = bf16[2048,512]{1,0:T(8,128)(2,1)} async-done(((bf16[64,512]{1,0:T(8,128)(2,1)}), bf16[2048,512]{1,0:T(8,128)(2,1)}) %all-gather.9.cloned.1.call-update) | async-done | bytes 2097168 | tf_op jit(solution)/shard_map/all_gather | solution.py:30
  150.8 1.8 convolution_convert_fusion.4
  152.7 1.7 collective-permute-start
  174.2 1.5 pad.227
  177.4 40.9 %all-gather.2 = f32[32,2,256]{2,1,0:T(2,128)S(1)} all-gather(f32[1,2,256]{2,1,0:T(2,128)S(1)} %maximum_bitcast_fusion), channel_id=2, replica_groups=mesh['grp'=2,'sp'=32,'tp'=8] {'sp'}, dimensions={0}, use_global_device_ids=true | all-gather | bytes 67584 | tf_op jit(solution)/shard_map/all_gather | solution.py:48
  218.4 59.8 %all-gather.11.cloned.1.call-done = bf16[32,256,64]{1,2,0:T(8,128)(2,1)} async-done(((bf16[1,256,64]{1,2,0:T(8,128)(2,1)}), bf16[32,256,64]{1,2,0:T(8,128)(2,1)}) %all-gather.11.cloned.1.call-update) | async-done | bytes 1048592 | tf_op jit(solution)/shard_map/all_gather | solution.py:98
  278.2 3.8 convolution_convert_fusion.1
  282.1 46.2 %all_to_all.26 = bf16[8,384,256]{2,1,0:T(8,128)(2,1)S(1)} all-to-all(bf16[8,384,256]{2,1,0:T(8,128)(2,1)S(1)} %bitcast.110), channel_id=1, replica_groups=mesh['grp'=2,'sp'=32,'tp'=8] {'tp'}, dimensions={0} | all-to-all | bytes 3145728 | tf_op jit(solution)/shard_map/all_to_all | solution.py:77
  329.5 1.3 broadcast_in_dim.7
  330.8 4.5 all-to-all-start.2
  335.9 20.1 %all-to-all-done.2 = bf16[8,384,256]{1,2,0:T(8,128)(2,1)S(1)} async-done(((bf16[8,384,256]{1,2,0:T(8,128)(2,1)}), bf16[8,384,256]{1,2,0:T(8,128)(2,1)S(1)}, u32[]{:S(2)}, u32[]{:S(2)}) %all-to-all-start.2) | async-done | bytes 1572896 | tf_op jit(solution)/shard_map/all_to_all | solution.py:13
  356.9 52.8 %all-gather.13.cloned.1.call-done = bf16[2048,512]{1,0:T(8,128)(2,1)} async-done(((bf16[64,512]{1,0:T(8,128)(2,1)}), bf16[2048,512]{1,0:T(8,128)(2,1)}) %all-gather.13.cloned.1.call-update) | async-done | bytes 2097168 | tf_op jit(solution)/shard_map/all_gather | solution.py:30
  409.7 1.8 convolution_convert_fusion.2
  411.6 1.5 collective-permute-start.1
  414.2 1.3 fusion.22
  415.9 0.8 slice.719
  416.7 1.0 multiply_add_fusion.2
  440.9 0.8 fusion.103
  443.3 1.6 pad.259
  446.4 1.7 pad.242
  448.8 41.6 %all-gather.3 = f32[32,2,256]{2,1,0:T(2,128)S(1)} all-gather(f32[1,2,256]{2,1,0:T(2,128)S(1)} %maximum_bitcast_fusion.1), channel_id=3, replica_groups=mesh['grp'=2,'sp'=32,'tp'=8] {'sp'}, dimensions={0}, use_global_device_ids=true | all-gather | bytes 67584 | tf_op jit(solution)/shard_map/all_gather | solution.py:48
  490.5 45.1 %all-gather.15.cloned.1.call-done = bf16[32,256,64]{1,2,0:T(8,128)(2,1)} async-done(((bf16[1,256,64]{1,2,0:T(8,128)(2,1)}), bf16[32,256,64]{1,2,0:T(8,128)(2,1)}) %all-gather.15.cloned.1.call-update) | async-done | bytes 1048592 | tf_op jit(solution)/shard_map/all_gather | solution.py:98
  535.7 3.9 convolution_convert_fusion
  539.7 46.7 %all_to_all.27 = bf16[8,384,256]{2,1,0:T(8,128)(2,1)S(1)} all-to-all(bf16[8,384,256]{2,1,0:T(8,128)(2,1)S(1)} %bitcast.111), channel_id=1, replica_groups=mesh['grp'=2,'sp'=32,'tp'=8] {'tp'}, dimensions={0} | all-to-all | bytes 3145728 | tf_op jit(solution)/shard_map/all_to_all | solution.py:77
  586.7 8.1 %all_to_all.28 = f32[8,1,384]{2,1,0:T(1,128)S(1)} all-to-all(f32[8,1,384]{2,1,0:T(1,128)S(1)} %broadcast_in_dim.8), channel_id=1, replica_groups=mesh['grp'=2,'sp'=32,'tp'=8] {'tp'}, dimensions={0} | all-to-all | bytes 24576 | tf_op jit(solution)/shard_map/all_to_all | solution.py:13
  594.9 0.8 fusion.34
  (388 shorter events, 55.8 us)
Async XLA Ops:
  6.5 144.2 %all-gather.9.cloned.1.call-start = ((), (), s32[]{:S(2)}) async-start(), calls=%async_computation.5 | async-start | bytes 2162688 | tf_op jit(solution)/shard_map/all_gather | solution.py:30
  8.1 270.1 %all-gather.11.cloned.1.call-start = ((), (), s32[]{:S(2)}) async-start(), calls=%async_computation.6 | async-start | bytes 1081344 | tf_op jit(solution)/shard_map/all_gather | solution.py:98
  12.0 45.8 %copy-start.28 = (f32[2,256]{1,0:T(2,128)S(1)}, f32[2,256]{1,0:T(2,128)}, u32[]{:S(2)}) copy-start(f32[2,256]{1,0:T(2,128)} %param.22) | copy-start | bytes 6148
  12.0 46.4 %copy-start.11 = (bf16[2,4,256]{2,1,0:T(4,128)(2,1)S(1)}, bf16[2,4,256]{2,1,0:T(4,128)(2,1)}, u32[]{:S(2)}) copy-start(bf16[2,4,256]{2,1,0:T(4,128)(2,1)} %param.19) | copy-start | bytes 12292
  12.0 47.0 %copy-start.10 = (f32[2,2048]{1,0:T(2,128)S(1)}, f32[2,2048]{1,0:T(2,128)}, u32[]{:S(2)}) copy-start(f32[2,2048]{1,0:T(2,128)} %param.26) | copy-start | bytes 49156
  12.0 65.7 %all-to-all-start = ((bf16[8,384,256]{1,2,0:T(8,128)(2,1)}), bf16[8,384,256]{1,2,0:T(8,128)(2,1)S(1)}, u32[]{:S(2)}, u32[]{:S(2)}) async-start(bf16[8,384,256]{1,2,0:T(8,128)(2,1)} %broadcast_in_dim.6), calls=%async_computation | async-start | bytes 3145728 | tf_op jit(solution)/shard_map/all_to_all | solution.py:13
  57.1 352.6 %all-gather.13.cloned.1.call-start = ((), (), s32[]{:S(2)}) async-start(), calls=%async_computation.7 | async-start | bytes 2162688 | tf_op jit(solution)/shard_map/all_gather | solution.py:30
  78.6 76.7 %copy-start.31 = (f32[384,256]{1,0:T(8,128)S(1)}, f32[384,256]{1,0:T(8,128)}, u32[]{:S(2)}) copy-start(f32[384,256]{1,0:T(8,128)} %param.24) | copy-start | bytes 1179652
  78.6 76.7 %copy-start.33 = (bf16[2,1,256,256]{3,2,1,0:T(8,128)(2,1)S(1)}, bf16[2,1,256,256]{3,2,1,0:T(8,128)(2,1)}, u32[]{:S(2)}) copy-start(bf16[2,1,256,256]{3,2,1,0:T(8,128)(2,1)} %param.20) | copy-start | bytes 786436
  78.6 76.7 %copy-start.36 = (f32[384]{0:T(512)S(1)}, f32[384]{0:T(512)}, u32[]{:S(2)}) copy-start(f32[384]{0:T(512)} %param.23) | copy-start | bytes 4612
  152.7 2.5 collective-permute-start
  156.1 11.2 %copy-start = (f32[384,256]{1,0:T(8,128)}, f32[384,256]{1,0:T(8,128)S(1)}, u32[]{:S(2)}) copy-start(f32[384,256]{1,0:T(8,128)S(1)} %fusion.25) | copy-start | bytes 1179652
  176.5 101.7 %copy-start.5 = (f32[384,256]{1,0:T(8,128)}, f32[384,256]{1,0:T(8,128)S(1)}, u32[]{:S(2)}) copy-start(f32[384,256]{1,0:T(8,128)S(1)} %pad.226) | copy-start | bytes 1179652
  177.2 101.0 %copy-start.6 = (f32[384,256]{1,0:T(8,128)}, f32[384,256]{1,0:T(8,128)S(1)}, u32[]{:S(2)}) copy-start(f32[384,256]{1,0:T(8,128)S(1)} %pad.211) | copy-start | bytes 1179652
  330.8 25.2 %all-to-all-start.2 = ((bf16[8,384,256]{1,2,0:T(8,128)(2,1)}), bf16[8,384,256]{1,2,0:T(8,128)(2,1)S(1)}, u32[]{:S(2)}, u32[]{:S(2)}) async-start(bf16[8,384,256]{1,2,0:T(8,128)(2,1)} %broadcast_in_dim.7), calls=%async_computation.2 | async-start | bytes 3145728 | tf_op jit(solution)/shard_map/all_to_all | solution.py:13
  335.3 200.3 %all-gather.15.cloned.1.call-start = ((), (), s32[]{:S(2)}) async-start(), calls=%async_computation.8 | async-start | bytes 1081344 | tf_op jit(solution)/shard_map/all_gather | solution.py:98
  356.8 56.7 %copy-start.12 = (f32[1,1,256]{2,1,0:T(1,128)S(1)}, f32[1,1,256]{2,1,0:T(1,128)}, u32[]{:S(2)}) copy-start(f32[1,1,256]{2,1,0:T(1,128)} %get-tuple-element.193) | copy-start | bytes 3076
  356.9 56.7 %copy-start.13 = (f32[1,1,256]{2,1,0:T(1,128)S(1)}, f32[1,1,256]{2,1,0:T(1,128)}, u32[]{:S(2)}) copy-start(f32[1,1,256]{2,1,0:T(1,128)} %get-tuple-element.194) | copy-start | bytes 3076
  356.9 56.7 %copy-start.14 = (f32[1,1,256]{2,1,0:T(1,128)S(1)}, f32[1,1,256]{2,1,0:T(1,128)}, u32[]{:S(2)}) copy-start(f32[1,1,256]{2,1,0:T(1,128)} %get-tuple-element.199) | copy-start | bytes 3076
  356.9 56.7 %copy-start.15 = (f32[1,1,256]{2,1,0:T(1,128)S(1)}, f32[1,1,256]{2,1,0:T(1,128)}, u32[]{:S(2)}) copy-start(f32[1,1,256]{2,1,0:T(1,128)} %get-tuple-element.200) | copy-start | bytes 3076
  356.9 56.9 %copy-start.30 = (f32[1,256]{1,0:T(1,128)S(1)}, f32[1,256]{1,0:T(1,128)}, u32[]{:S(2)}) copy-start(f32[1,256]{1,0:T(1,128)} %get-tuple-element.209) | copy-start | bytes 3076
  356.9 56.9 %copy-start.32 = (f32[384,256]{1,0:T(8,128)S(1)}, f32[384,256]{1,0:T(8,128)}, u32[]{:S(2)}) copy-start(f32[384,256]{1,0:T(8,128)} %param.24) | copy-start | bytes 1179652
  356.9 56.9 %copy-start.34 = (bf16[2,1,256,256]{3,2,1,0:T(8,128)(2,1)S(1)}, bf16[2,1,256,256]{3,2,1,0:T(8,128)(2,1)}, u32[]{:S(2)}) copy-start(bf16[2,1,256,256]{3,2,1,0:T(8,128)(2,1)} %param.20) | copy-start | bytes 786436
  356.9 56.9 %copy-start.37 = (f32[384]{0:T(512)S(1)}, f32[384]{0:T(512)}, u32[]{:S(2)}) copy-start(f32[384]{0:T(512)} %param.23) | copy-start | bytes 4612
  411.6 2.0 collective-permute-start.1
  415.5 18.7 %copy-start.1 = (f32[384,256]{1,0:T(8,128)}, f32[384,256]{1,0:T(8,128)S(1)}, u32[]{:S(2)}) copy-start(f32[384,256]{1,0:T(8,128)S(1)} %fusion.22) | copy-start | bytes 1179652
  432.5 8.2 %copy-start.25 = (f32[1,256]{1,0:T(1,128)S(1)}, f32[1,256]{1,0:T(1,128)}, u32[]{:S(2)}) copy-start(f32[1,256]{1,0:T(1,128)} %slice.887) | copy-start | bytes 3076
  432.5 8.3 %copy-start.23 = (f32[1,256]{1,0:T(1,128)S(1)}, f32[1,256]{1,0:T(1,128)}, u32[]{:S(2)}) copy-start(f32[1,256]{1,0:T(1,128)} %slice.861) | copy-start | bytes 3076
  432.5 8.4 %copy-start.7 = (f32[47,256]{1,0:T(8,128)S(1)}, f32[47,256]{1,0:T(8,128)}, u32[]{:S(2)}) copy-start(f32[47,256]{1,0:T(8,128)} %slice.769) | copy-start | bytes 144388
  445.6 90.0 %copy-start.3 = (f32[384,256]{1,0:T(8,128)}, f32[384,256]{1,0:T(8,128)S(1)}, u32[]{:S(2)}) copy-start(f32[384,256]{1,0:T(8,128)S(1)} %pad.258) | copy-start | bytes 1179652
  446.4 89.3 %copy-start.4 = (f32[384,256]{1,0:T(8,128)}, f32[384,256]{1,0:T(8,128)S(1)}, u32[]{:S(2)}) copy-start(f32[384,256]{1,0:T(8,128)S(1)} %pad.243) | copy-start | bytes 1179652
  586.3 8.5 %copy-start.29 = (f32[256]{0:T(256)S(1)}, f32[256]{0:T(256)}, u32[]{:S(2)}) copy-start(f32[256]{0:T(256)} %param.27) | copy-start | bytes 3076
  (16 other events, 60.6 us)
Sparse Core Ops, SparseCore 0:
  9.4 141.3 all-gather.8
  152.9 125.2 all-gather.10
  280.3 129.3 all-gather.12
  411.6 123.9 all-gather.14
